TPU v7x, 32 devices: a whole 2x2x4 slice. The times are simulated.
32 devices in a mesh: sp: 16 (over z, y, x), tp: 2 (over core).
Axes of the slice: x: 2, y: 2, z: 4, core: 2. Of those that a mesh axis runs over, the one named last changes fastest.
Arguments:
- stream: bfloat16 [8192, 2048], P(('sp', 'tp')), may hold values from -6 to 6
- queries: bfloat16 [8192, 512], P('sp', 'tp'), may hold values from -6 to 6
- key_rows: bfloat16 [8192, 512], P('sp', 'tp'), may hold values from -6 to 6
- value_rows: bfloat16 [8192, 1024], P('sp', 'tp'), may hold values from -6 to 6
- out_gate: bfloat16 [8192, 1024], P('sp', 'tp'), may hold values from -6 to 6
- in_gate: float32 [4, 8192], P('tp', 'sp'), may hold values from -4 to 214
- forget_gate: float32 [4, 8192], P('tp', 'sp'), may hold values from -2 to 20
- out_proj: bfloat16 [1024, 2048], replicated, may hold values from -0.1875 to 0.1875
- ffn_gain: float32 [2048], replicated, may hold values from 0.1 to 1.9
- gate_proj: bfloat16 [16, 2048, 768], P('sp', None, 'tp'), may hold values from -0.125 to 0.125
- up_proj: bfloat16 [16, 2048, 768], P('sp', None, 'tp'), may hold values from -0.125 to 0.125
- down_proj: bfloat16 [16, 768, 2048], P('sp', 'tp'), may hold values from -0.21875 to 0.21875
- expert_ids: int32 [8192, 2], P(('sp', 'tp')), may hold values from 0 to 15, as said below
- route_weights: float32 [8192, 2], P(('sp', 'tp')), may hold values from 0.05 to 1
Outputs:
- result_stream: bfloat16 [8192, 2048], P(('sp', 'tp'))
Inputs may be any that keep to these rules, and one draw needn't show every extreme that they name: `expert_ids`: both experts of a row are different and lie in one group (expert // 8 equal). In the rows of one device (aligned blocks of 256 rows) each expert is named at most 64 times, some expert exactly 64 times, and each expert shares its rows with a single partner.
All inputs are finite; a program needn't handle non-finite values.
Results may differ from a plain program's by a relative error of at most 0.012.
Values may be sent and summed in bfloat16 or wider, within the bound.
A program may use at most 128 MiB of HBM per device.

v0:
```python
import jax
import jax.numpy as jnp
from jax import lax
from jax.sharding import PartitionSpec as P

QK = 128
V_DIM = 256
BLOCK = 64


epsilon = 1e-06
floor_level = -1e30


def carried_in(value, axis, join, neutral):
    count, mine = (lax.axis_size(axis), lax.axis_index(axis))
    pieces = jax.tree.map(lambda part: lax.all_gather(part, axis), value)
    total = jax.tree.map(
        lambda part, zero: jnp.full_like(part, 0) + jnp.asarray(zero, part.dtype), value, neutral
    )

    def turn(position, total):
        longer = join(total, jax.tree.map(lambda part: part[position], pieces))
        return jax.tree.map(lambda new, old: jnp.where(position < mine, new, old), longer, total)

    return lax.fori_loop(0, count - 1, turn, total)


def join_states(earlier, later):
    early_state, early_level, early_decay = earlier
    late_state, late_level, late_decay = later
    level = jnp.maximum(late_decay + early_level, late_level)
    state = (
        early_state * jnp.exp(late_decay + early_level - level)[:, None, None]
        + late_state * jnp.exp(late_level - level)[:, None, None]
    )
    return (state, level, early_decay + late_decay)


def body(
    stream,
    queries,
    key_rows,
    value_rows,
    out_gate,
    in_gate,
    forget_gate,
    out_proj,
    ffn_gain,
    gate_proj,
    up_proj,
    down_proj,
    expert_ids,
    route_weights,
):
    heads_here, length = in_gate.shape
    blocks = length // BLOCK

    def per_head(rows, size):
        return (
            rows.astype(jnp.float32).reshape(blocks, BLOCK, heads_here, size).transpose(2, 0, 1, 3)
        )

    query_blocks = per_head(queries, QK)
    key_blocks = per_head(key_rows, QK) * QK ** (-0.5)
    value_blocks = per_head(value_rows, V_DIM)
    input_gate = in_gate.reshape(heads_here, blocks, BLOCK)
    cumulative = jnp.cumsum(
        jax.nn.log_sigmoid(forget_gate).reshape(heads_here, blocks, BLOCK), axis=-1
    )
    closing = cumulative[..., -1]
    causal = jnp.tril(jnp.ones((BLOCK, BLOCK), dtype=bool))
    log_inner = jnp.where(
        causal,
        cumulative[..., :, None] - cumulative[..., None, :] + input_gate[..., None, :],
        -jnp.inf,
    )
    log_close = closing[..., None] - cumulative + input_gate

    def advance(carry, inputs):
        state, level, decay = carry
        key_block, value_block, close_block, last_block = inputs
        new_level = jnp.maximum(last_block + level, jnp.max(close_block, axis=-1))
        weight = jnp.exp(close_block - new_level[:, None])
        update = jnp.einsum(
            "hl,hld,hle->hde", weight, key_block, value_block, precision=lax.Precision.HIGHEST
        )
        new_state = state * jnp.exp(last_block + level - new_level)[:, None, None] + update
        return ((new_state, new_level, decay + last_block), (state, level, decay))

    empty = (
        jnp.zeros((heads_here, QK, V_DIM), jnp.float32),
        jnp.full((heads_here,), floor_level, jnp.float32),
        jnp.zeros((heads_here,), jnp.float32),
    )
    summary, before = lax.scan(
        advance,
        empty,
        (
            jnp.moveaxis(key_blocks, 1, 0),
            jnp.moveaxis(value_blocks, 1, 0),
            jnp.moveaxis(log_close, 1, 0),
            closing.T,
        ),
    )
    carried = carried_in(summary, "sp", join_states, empty)
    anchor = join_states(
        (
            jnp.zeros((heads_here, QK, V_DIM), jnp.float32),
            jnp.zeros((heads_here,), jnp.float32),
            jnp.zeros((heads_here,), jnp.float32),
        ),
        carried,
    )
    anchor_state, anchor_level, _ = anchor
    block_states, block_levels, block_decays = before
    levels = jnp.maximum(block_decays + anchor_level[None, :], block_levels)
    states = (
        anchor_state[None] * jnp.exp(block_decays + anchor_level[None, :] - levels)[..., None, None]
        + block_states * jnp.exp(block_levels - levels)[..., None, None]
    )
    states = jnp.moveaxis(states, 0, 1)
    levels = levels.T
    log_inter = cumulative + levels[..., None]
    peak = jnp.maximum(log_inter, jnp.max(log_inner, axis=-1))
    scores = jnp.einsum(
        "hntd,hnsd->hnts", query_blocks, key_blocks, precision=lax.Precision.HIGHEST
    ) * jnp.exp(log_inner - peak[..., None])
    from_state = jnp.einsum(
        "hntd,hnde->hnte", query_blocks, states, precision=lax.Precision.HIGHEST
    )
    from_block = jnp.einsum(
        "hnts,hnse->hnte", scores, value_blocks, precision=lax.Precision.HIGHEST
    )
    numerator = jnp.exp(log_inter - peak)[..., None] * from_state + from_block
    numerator = numerator.transpose(1, 2, 0, 3).reshape(length, heads_here, V_DIM)
    scaled = numerator * lax.rsqrt(
        jnp.mean(numerator * numerator, axis=-1, keepdims=True) + epsilon
    )
    gated = scaled.reshape(length, heads_here * V_DIM) * jax.nn.sigmoid(
        out_gate.astype(jnp.float32)
    )
    heads_out = gated.astype(jnp.bfloat16)
    rows_here, model_width = stream.shape
    token_heads = lax.all_to_all(heads_out, "tp", split_axis=0, concat_axis=1, tiled=True)
    mix = jnp.dot(token_heads, out_proj, preferred_element_type=jnp.float32)
    middle = (stream.astype(jnp.float32) + mix).astype(jnp.bfloat16)
    middle_float = middle.astype(jnp.float32)
    normed = (
        middle_float
        * lax.rsqrt(jnp.mean(middle_float * middle_float, axis=-1, keepdims=True) + epsilon)
        * ffn_gain
    ).astype(jnp.bfloat16)
    experts_total = lax.axis_size("sp")
    per_token = expert_ids.shape[1]
    capacity = 2 * per_token * rows_here // experts_total
    flat_ids = expert_ids.reshape(-1)
    onehot = (flat_ids[:, None] == jnp.arange(experts_total, dtype=jnp.int32)[None, :]).astype(
        jnp.int32
    )
    slot_rank = jnp.sum((jnp.cumsum(onehot, axis=0) - onehot) * onehot, axis=1)
    slot_index = flat_ids * capacity + slot_rank
    owners = (
        jnp.zeros((experts_total * capacity,), jnp.int32)
        .at[slot_index]
        .set(jnp.arange(rows_here * per_token, dtype=jnp.int32) // per_token)
    )
    filled = jnp.zeros((experts_total * capacity,), jnp.bfloat16).at[slot_index].set(1)
    outgoing = (normed[owners] * filled[:, None]).reshape(experts_total, capacity, model_width)
    gate_full, up_full, down_full = (
        lax.all_gather(gate_proj[0], "tp", axis=1, tiled=True),
        lax.all_gather(up_proj[0], "tp", axis=1, tiled=True),
        lax.all_gather(down_proj[0], "tp", axis=0, tiled=True),
    )
    arrived = lax.all_to_all(outgoing, "sp", split_axis=0, concat_axis=0, tiled=True)
    sources, amount, _ = arrived.shape
    flattened = arrived.reshape(sources * amount, model_width)
    hidden = (
        jax.nn.silu(jnp.dot(flattened, gate_full, preferred_element_type=jnp.float32))
        * jnp.dot(flattened, up_full, preferred_element_type=jnp.float32)
    ).astype(jnp.bfloat16)
    returned = lax.all_to_all(
        jnp.dot(hidden, down_full, preferred_element_type=jnp.float32)
        .astype(jnp.bfloat16)
        .reshape(sources, amount, model_width),
        "sp",
        split_axis=0,
        concat_axis=0,
        tiled=True,
    )
    picked = (
        returned.reshape(experts_total * capacity, model_width)[slot_index]
        .reshape(rows_here, per_token, model_width)
        .astype(jnp.float32)
    )
    expert_sum = jnp.sum(picked * route_weights[..., None], axis=1)
    return (middle_float + expert_sum).astype(jnp.bfloat16)


def solution(mesh):
    in_specs = (
        P(("sp", "tp"), None),
        P("sp", "tp"),
        P("sp", "tp"),
        P("sp", "tp"),
        P("sp", "tp"),
        P("tp", "sp"),
        P("tp", "sp"),
        P(),
        P(),
        P("sp", None, "tp"),
        P("sp", None, "tp"),
        P("sp", "tp", None),
        P(("sp", "tp"), None),
        P(("sp", "tp"), None),
    )
    out_specs = P(("sp", "tp"), None)
    return jax.shard_map(body, mesh=mesh, in_specs=in_specs, out_specs=out_specs, check_vma=False)
```

profile of v0, /device:TPU:14, one launch (start us, length us, event | category | flops | bytes accessed | tf_op | source)
XLA Modules:
  0.0 395.5 jit_solution(13375230313949620442)
XLA Ops:
  6.5 0.7 fusion.50
  7.9 0.8 reshape.148
  8.9 1.2 reshape.149
  10.4 1.0 convert_multiply_fusion.2
  11.7 12.8 %while.39 = (s32[]{:T(128)}, f32[2,128,256]{2,1,0:T(8,128)S(1)}, f32[2]{0:T(128)S(1)}, f32[2]{0:T(128)S(1)}, f32[8,2,128,256]{3,2,1,0:T(8,128)}, /*index=5*/f32[...) while((s32[]{:T(128)}, f32[2,128,256]{2,1,0:T(8,128)S(1)}, ...), condition=%wide.region_3.4_spmd.clone, body=%wide.region_1.3_spmd.clone.sunk | while | flops 50610444 | bytes 1642301 | solution.py:96
  12.0 0.7 bitcast_dynamic-update-slice_fusion.2
  12.7 0.5 convolution_add_fusion.3
  13.6 0.7 bitcast_dynamic-update-slice_fusion.2
  14.3 0.5 convolution_add_fusion.3
  15.1 0.7 bitcast_dynamic-update-slice_fusion.2
  16.7 0.7 bitcast_dynamic-update-slice_fusion.2
  17.5 0.5 convolution_add_fusion.3
  18.4 0.7 bitcast_dynamic-update-slice_fusion.2
  20.0 0.7 bitcast_dynamic-update-slice_fusion.2
  20.8 0.5 convolution_add_fusion.3
  21.6 0.7 bitcast_dynamic-update-slice_fusion.2
  22.3 0.5 convolution_add_fusion.3
  23.2 0.7 bitcast_dynamic-update-slice_fusion.2
  24.6 0.7 copy-done
  25.3 0.7 all-gather.15.cloned.1.call-update
  26.6 0.7 dynamic-slice
  28.4 29.4 %all-reduce.2 = (f32[32]{0:T(128)S(1)}, f32[32]{0:T(128)S(1)}) all-reduce(f32[32]{0:T(128)S(1)} %dynamic-update-slice, f32[32]{0:T(128)S(1)} %dynamic-update-slice.1), channel_id=2, replica_groups=mesh['sp'=16,'tp'=2] {'sp'}, use_global_device_ids=true, to_apply=%add | all-reduce | flops 64 | bytes 512
  58.3 0.8 reshape.150
  59.1 1.1 reduce-window.6
  60.9 2.4 scatter_custom_fusion
  63.3 3.9 scatter_custom_fusion.1
  67.4 33.9 %all-gather.11.cloned.1.call-done = f32[32,128,256]{2,1,0:T(8,128)} async-done(((f32[2,128,256]{2,1,0:T(8,128)}), f32[32,128,256]{2,1,0:T(8,128)}) %all-gather.11.cloned.1.call-update) | async-done | bytes 4194320 | tf_op jit(solution)/shard_map/all_gather | solution.py:17
  101.3 17.3 %while.40 = (s32[]{:T(128)}, f32[2,128,256]{2,1,0:T(8,128)S(1)}, f32[2]{0:T(128)S(1)}, f32[2]{0:T(128)S(1)}, s32[]{:T(128)}, /*index=5*/f32[16,2]{1,0:T(8,128)S(...) while((s32[]{:T(128)}, f32[2,128,256]{2,1,0:T(8,128)S(1)}, ...), condition=%wide.region_5.6_spmd.clone, body=%wide.region_4.5_spmd.clone.sunk | while | flops 327704 | bytes 786671 | solution.py:26
  101.3 1.2 fusion.70
  102.6 1.1 fusion.70
  103.7 1.1 fusion.70
  104.8 1.1 fusion.70
  106.0 1.1 fusion.70
  107.1 1.1 fusion.70
  108.2 1.1 fusion.70
  109.4 1.1 fusion.70
  110.6 1.1 fusion.70
  111.7 1.1 fusion.70
  112.9 1.1 fusion.70
  114.0 1.1 fusion.70
  115.2 1.1 fusion.70
  116.3 1.1 fusion.70
  117.4 1.1 fusion.70
  118.9 1.5 fusion.34
  120.5 2.1 fusion.31
  122.7 0.8 multiply_reduce_fusion.1
  123.6 0.6 mul.210
  124.3 0.8 copy.50
  125.9 4.2 %all_to_all.29 = bf16[2,256,512]{1,2,0:T(8,128)(2,1)S(1)} all-to-all(bf16[2,256,512]{1,2,0:T(8,128)(2,1)S(1)} %copy.52), channel_id=1, replica_groups=mesh['sp'=16,'tp'=2] {'tp'}, dimensions={0} | all-to-all | bytes 1048576 | tf_op jit(solution)/shard_map/all_to_all | solution.py:145
  130.1 3.6 fusion.21
  133.7 1.0 copy-done.1
  135.0 6.1 %gather_fusion = bf16[1024,2048]{1,0:T(8,128)(2,1)} fusion(bf16[256,2048]{1,0:T(8,128)(2,1)S(1)} %fusion.23, s32[1024]{0:T(1024)S(1)} %fusion.49), kind=kCustom, calls=%fused_computation | custom fusion | bytes 8392704 | tf_op jit(solution)/shard_map/gather | solution.py:169
  141.1 4.5 %broadcast_multiply_fusion = bf16[16,64,2048]{2,1,0:T(8,128)(2,1)} fusion(bf16[16,64,2048]{2,1,0:T(8,128)(2,1)} %bitcast.153, bf16[16,64]{1,0:T(8,128)(2,1)S(1)} %mul.223), kind=kLoop, calls=%fused_computation.56 | loop fusion | flops 2097152 | bytes 8390656 | tf_op jit(solution)/shard_map/mul | solution.py:169
  145.6 5.8 %all-to-all-start.1 = ((bf16[16,64,2048]{2,1,0:T(8,128)(2,1)}), bf16[16,64,2048]{2,1,0:T(8,128)(2,1)}, u32[]{:S(2)}, u32[]{:S(2)}) async-start(bf16[16,64,2048]{2,1,0:T(8,128)(2,1)} %broadcast_multiply_fusion), calls=%async_computation.1 | async-start | bytes 8388608 | tf_op jit(solution)/shard_map/all_to_all | solution.py:175
  151.4 0.7 all-gather.13.cloned.1.call-update
  152.7 94.7 %all-to-all-done.1 = bf16[16,64,2048]{2,1,0:T(8,128)(2,1)} async-done(((bf16[16,64,2048]{2,1,0:T(8,128)(2,1)}), bf16[16,64,2048]{2,1,0:T(8,128)(2,1)}, u32[]{:S(2)}, u32[]{:S(2)}) %all-to-all-start.1) | async-done | bytes 4194336 | tf_op jit(solution)/shard_map/all_to_all | solution.py:175
  247.4 8.2 %fusion.14 = f32[1024,768]{1,0:T(8,128)} fusion(bf16[1024,2048]{1,0:T(8,128)(2,1)} %bitcast.24, bf16[1,2048,768]{2,1,0:T(8,128)(2,1)} %all-gather.15.cloned.1.call-done), kind=kOutput, calls=%fused_computation.40 | convolution fusion | flops 3221225472 | bytes 10485760 | tf_op jit(solution)/shard_map/dot_general | solution.py:180
  255.6 13.2 %convolution_convert_fusion = bf16[1024,2048]{1,0:T(8,128)(2,1)} fusion(bf16[1,768,2048]{2,1,0:T(8,128)(2,1)} %all-gather.17.cloned.1.call-done, f32[1024,768]{1,0:T(8,128)} %fusion.14, bf16[1024,2048]{1,0:T(8,128)(2,1)} %bitcast.24, bf16[1,2048,768]{2,1,0:T(8,128)(2,1)} %all-gather.13.cloned.1.call-done), kind=kOutput, calls=%fused_computation.38 | convolution fusion | flops 6449266688 | bytes 17825792 | tf_op jit(solution)/shard_map/dot_general | solution.py:183
  268.8 5.5 %all-to-all-start.2 = ((bf16[16,64,2048]{2,1,0:T(8,128)(2,1)}), bf16[16,64,2048]{2,1,0:T(8,128)(2,1)}, u32[]{:S(2)}, u32[]{:S(2)}) async-start(bf16[16,64,2048]{2,1,0:T(8,128)(2,1)} %bitcast.158), calls=%async_computation.2 | async-start | bytes 8388608 | tf_op jit(solution)/shard_map/all_to_all | solution.py:182
  274.5 93.0 %all-to-all-done.2 = bf16[16,64,2048]{2,1,0:T(8,128)(2,1)} async-done(((bf16[16,64,2048]{2,1,0:T(8,128)(2,1)}), bf16[16,64,2048]{2,1,0:T(8,128)(2,1)}, u32[]{:S(2)}, u32[]{:S(2)}) %all-to-all-start.2) | async-done | bytes 4194336 | tf_op jit(solution)/shard_map/all_to_all | solution.py:182
  367.6 7.1 %gather_fusion.1 = bf16[512,2048]{1,0:T(8,128)(2,1)S(1)} fusion(bf16[1024,2048]{1,0:T(8,128)(2,1)} %bitcast.29, s32[1024]{0:T(1024)S(1)} %pad_clamp_fusion), kind=kCustom, calls=%fused_computation.1 | custom fusion | bytes 4196352 | tf_op jit(solution)/shard_map/gather | solution.py:192
  374.7 4.0 %reshape.156 = f32[256,2,2048]{2,1,0:T(2,128)} reshape(bf16[512,2048]{1,0:T(8,128)(2,1)S(1)} %gather_fusion.1) | data formatting | bytes 6291456 | tf_op jit(solution)/shard_map/convert_element_type | solution.py:194
  378.7 9.0 %multiply_reduce_fusion = f32[256,2048]{1,0:T(8,128)S(1)} fusion(f32[256,2,2048]{2,1,0:T(2,128)} %reshape.156, f32[256,2]{1,0:T(8,128)S(1)} %copy.57), kind=kLoop, calls=%fused_computation.37 | loop fusion | flops 1572864 | bytes 6293504 | tf_op jit(solution)/shard_map/reduce_sum | solution.py:196
  387.7 1.3 fusion.24
  (193 shorter events, 10.8 us)
Async XLA Ops:
  6.5 94.7 %all-gather.11.cloned.1.call-start = ((), (), s32[]{:S(2)}) async-start(), calls=%async_computation.3 | async-start | bytes 4456448 | tf_op jit(solution)/shard_map/all_gather | solution.py:17
  11.7 14.4 %copy-start.7 = (s32[256,2]{0,1:T(2,128)S(1)}, s32[256,2]{0,1:T(2,128)}, u32[]{:S(2)}) copy-start(s32[256,2]{0,1:T(2,128)} %param.30) | copy-start | bytes 6148
  11.7 14.9 %copy-start.10 = (u32[32]{0:T(128)S(1)}, u32[32]{0:T(128)}, u32[]{:S(2)}) copy-start(u32[32]{0:T(128)} %constant.120) | copy-start | bytes 388
  11.7 46.6 %copy-start.5 = (bf16[512,256]{1,0:T(8,128)(2,1)S(1)}, bf16[512,256]{1,0:T(8,128)(2,1)}, u32[]{:S(2)}) copy-start(bf16[512,256]{1,0:T(8,128)(2,1)} %param.19) | copy-start | bytes 786436
  24.5 0.7 copy-start
  25.3 127.5 %all-gather.15.cloned.1.call-start = ((), (), s32[]{:S(2)}) async-start(), calls=%async_computation.5 | async-start | bytes 4718592 | tf_op jit(solution)/shard_map/all_gather | solution.py:172
  101.3 19.3 %copy-start.3 = (f32[8,2,128,256]{3,2,1,0:T(8,128)S(1)}, f32[8,2,128,256]{3,2,1,0:T(8,128)}, u32[]{:S(2)}) copy-start(f32[8,2,128,256]{3,2,1,0:T(8,128)} %get-tuple-element.216) | copy-start | bytes 6291460
  124.2 1.0 copy-start.4
  125.2 4.8 %copy-start.9 = (bf16[256,2048]{1,0:T(8,128)(2,1)S(1)}, bf16[256,2048]{1,0:T(8,128)(2,1)}, u32[]{:S(2)}) copy-start(bf16[256,2048]{1,0:T(8,128)(2,1)} %param.18) | copy-start | bytes 3145732
  130.0 4.6 %copy-start.6 = (f32[2048]{0:T(1024)S(1)}, f32[2048]{0:T(1024)}, u32[]{:S(2)}) copy-start(f32[2048]{0:T(1024)} %param.26) | copy-start | bytes 24580
  133.7 1.0 copy-start.1
  145.6 101.8 %all-to-all-start.1 = ((bf16[16,64,2048]{2,1,0:T(8,128)(2,1)}), bf16[16,64,2048]{2,1,0:T(8,128)(2,1)}, u32[]{:S(2)}, u32[]{:S(2)}) async-start(bf16[16,64,2048]{2,1,0:T(8,128)(2,1)} %broadcast_multiply_fusion), calls=%async_computation.1 | async-start | bytes 8388608 | tf_op jit(solution)/shard_map/all_to_all | solution.py:175
  151.4 104.2 %all-gather.13.cloned.1.call-start = ((), (), s32[]{:S(2)}) async-start(), calls=%async_computation.4 | async-start | bytes 4718592 | tf_op jit(solution)/shard_map/all_gather | solution.py:171
  152.1 103.5 %all-gather.17.cloned.1.call-start = ((), (), s32[]{:S(2)}) async-start(), calls=%async_computation.6 | async-start | bytes 4718592 | tf_op jit(solution)/shard_map/all_gather | solution.py:173
  268.8 5.6 %copy-start.8 = (f32[256,2]{0,1:T(2,128)S(1)}, f32[256,2]{0,1:T(2,128)}, u32[]{:S(2)}) copy-start(f32[256,2]{0,1:T(2,128)} %param.31) | copy-start | bytes 6148
  268.8 98.7 %all-to-all-start.2 = ((bf16[16,64,2048]{2,1,0:T(8,128)(2,1)}), bf16[16,64,2048]{2,1,0:T(8,128)(2,1)}, u32[]{:S(2)}, u32[]{:S(2)}) async-start(bf16[16,64,2048]{2,1,0:T(8,128)(2,1)} %bitcast.158), calls=%async_computation.2 | async-start | bytes 8388608 | tf_op jit(solution)/shard_map/all_to_all | solution.py:182
  378.7 9.0 %copy-start.2 = (bf16[256,2048]{1,0:T(8,128)(2,1)S(1)}, bf16[256,2048]{1,0:T(8,128)(2,1)}, u32[]{:S(2)}) copy-start(bf16[256,2048]{1,0:T(8,128)(2,1)} %copy-done.1) | copy-start | bytes 3145732
Sparse Core Ops, SparseCore 0:
  25.4 75.8 all-gather.10
  102.8 11.8 all-gather.14
  153.7 13.1 all-gather.12
  168.4 13.2 all-gather.16
where the time goes:
time: 397 us; the launch traced here: 395 us
  waiting for transfers between devices  223 us (56%)
  other arithmetic  44.4 us (11%)
  local copies, waits for them, and re-layouts  34 us (9%)
  blocking collectives  33.5 us (8%)
  matrix products  33.4 us (8%)
  between operations  14.3 us (4%)
  starting transfers between devices  11.7 us (3%)
    all_to_all x1, waiting for transfers between devices, body(): lax.all_to_all(outgoing, 'sp', split_axis=0, concat_axis=0, tiled=True)  94.7 us
    all_to_all x1, waiting for transfers between devices, body(): lax.all_to_all(jnp.dot(hidden, down_full, preferred_element_type=jnp.floa...  93 us
    all_gather x1, waiting for transfers between devices, carried_in(): pieces = jax.tree.map(lambda part: lax.all_gather(part, axis), value)  33.9 us
    unnamed x1, blocking collectives  29.4 us
    select_n x30, other arithmetic, turn(): jnp.where(position < mine, new, old)  16.5 us
    dot_general x1, matrix products, body(): jnp.dot(hidden, down_full, preferred_element_type=jnp.float32)  13.2 us
    reduce_sum x1, other arithmetic, body(): expert_sum = jnp.sum(picked * route_weights[..., None], axis=1)  8.96 us
    dot_general x1, matrix products, body(): jnp.dot(flattened, up_full, preferred_element_type=jnp.float32)  8.24 us
  transfers between devices with their start and end apart: 6, of which 3 were waited for; matrix products, arithmetic and copies ran while one was open for 15% of the time, Pallas kernels for 0%

commit v1 on v0

v1 whole, which is shorter than its diff:
```python
import functools

import jax
import jax.numpy as jnp
from jax import lax
from jax.experimental import pallas as pl
from jax.experimental.pallas import tpu as pltpu
from jax.sharding import PartitionSpec as P

GROUP = 8
CUM = 64
epsilon = 1e-06
bf16, f32 = jnp.bfloat16, jnp.float32


def exchange_kernel(axis, group, count, kinds, *refs):
    ins, outs = refs[:count], refs[count : 2 * count]
    send, recv = refs[2 * count :]
    mine = lax.axis_index(axis)
    base = (mine // group) * group
    me = mine - base

    barrier = pltpu.get_barrier_semaphore()
    for step in range(1, group):
        peer = base + lax.rem(me + step, group)
        pl.semaphore_signal(barrier, inc=1, device_id={axis: peer}, device_id_type=pl.DeviceIdType.MESH)
    pl.semaphore_wait(barrier, group - 1)
    copies = []
    for step in range(1, group):
        to = lax.rem(me + step, group)
        for n in range(count):
            copy = pltpu.make_async_remote_copy(
                src_ref=ins[n].at[to] if kinds[n] == "slab" else ins[n],
                dst_ref=outs[n].at[me],
                send_sem=send.at[n, step],
                recv_sem=recv.at[n, step],
                device_id={axis: base + to},
                device_id_type=pl.DeviceIdType.MESH,
            )
            copy.start()
            copies.append(copy)
    for n in range(count):
        outs[n][me] = ins[n][me] if kinds[n] == "slab" else ins[n][...]
    for copy in copies:
        copy.wait()


def exchange(arrays, kinds, axis, group, collective_id, cost):
    count = len(arrays)
    out_shape = [
        jax.ShapeDtypeStruct(a.shape if kind == "slab" else (group,) + a.shape, a.dtype)
        for a, kind in zip(arrays, kinds)
    ]
    return pl.pallas_call(
        functools.partial(exchange_kernel, axis, group, count, kinds),
        out_shape=out_shape,
        in_specs=[pl.BlockSpec(memory_space=pltpu.VMEM)] * count,
        out_specs=[pl.BlockSpec(memory_space=pltpu.VMEM)] * count,
        scratch_shapes=[
            pltpu.SemaphoreType.DMA((count, group)),
            pltpu.SemaphoreType.DMA((count, group)),
        ],
        compiler_params=pltpu.CompilerParams(collective_id=collective_id, has_side_effects=True),
        cost_estimate=pl.CostEstimate(flops=0, bytes_accessed=cost, transcendentals=0),
    )(*arrays)


def device_prefix(state, level, decay):
    total, mine = lax.axis_size("sp"), lax.axis_index("sp")
    heads, qk, width = state.shape
    rows = heads * qk // total
    slabs = state.astype(bf16).reshape(total, rows, width)
    info = jnp.zeros((8, 128), f32).at[0, :heads].set(level).at[1, :heads].set(decay)
    slabs, infos = exchange((slabs, info), ("slab", "all"), "sp", total, 1, 10_000_000)
    levels, decays = infos[:, 0, :heads].T, infos[:, 1, :heads].T
    order = jnp.arange(total)
    between = (order[None, :, None] < order[None, None, :]) & (order[None, None, :] < order[:, None, None])
    gap = jnp.sum(jnp.where(between[None], decays[:, None, None, :], 0.0), axis=-1)
    earlier = order[None, :] < order[:, None]
    reach = jnp.where(earlier[None], levels[:, None, :] + gap, -jnp.inf)
    start = jnp.sum(jnp.where(earlier[None], decays[:, None, :], 0.0), axis=-1)
    top = jnp.maximum(start, jnp.max(reach, axis=-1))
    weights = jnp.exp(reach - top[..., None])
    head_here = mine * heads // total
    weight = lax.dynamic_index_in_dim(weights, head_here, 0, keepdims=False)
    prefix = jnp.dot(
        weight, slabs.astype(f32).reshape(total, rows * width), precision=lax.Precision.HIGHEST
    )
    prefix = prefix.astype(bf16).reshape(total, rows, width)
    (prefix,) = exchange((prefix,), ("slab",), "sp", total, 2, 10_000_000)
    top_mine = lax.dynamic_index_in_dim(top, mine, 1, keepdims=False)
    return prefix.reshape(heads, qk, width), top_mine


def mixer(queries, key_rows, value_rows, out_gate, in_gate, forget_gate):
    heads, length = in_gate.shape
    qk, width = queries.shape[1] // heads, value_rows.shape[1] // heads
    scale = qk ** (-0.5)
    q = queries.reshape(length, heads, qk)
    k = key_rows.reshape(length, heads, qk)
    v = value_rows.reshape(length, heads, width)
    pieces = jnp.cumsum(jax.nn.log_sigmoid(forget_gate).reshape(heads, length // CUM, CUM), axis=-1)
    closing = pieces[..., -1]
    before = jnp.cumsum(closing, axis=-1) - closing
    cumulative = (pieces + before[..., None]).reshape(heads, length)
    decay = cumulative[:, -1]
    log_close = decay[:, None] - cumulative + in_gate
    level = jnp.max(log_close, axis=-1)
    close = jnp.exp(log_close - level[:, None]) * scale
    weighted = (k.astype(f32) * close.T[:, :, None]).astype(bf16)
    state = jnp.einsum("lhd,lhe->hde", weighted, v, preferred_element_type=f32)
    carried, carried_level = device_prefix(state, level, decay)

    causal = jnp.tril(jnp.ones((length, length), dtype=bool))
    log_inner = jnp.where(
        causal, cumulative[:, :, None] + (in_gate - cumulative)[:, None, :], -jnp.inf
    )
    log_inter = cumulative + carried_level[:, None]
    peak = jnp.maximum(log_inter, jnp.max(log_inner, axis=-1))
    scores = jnp.einsum("thd,shd->hts", q, k, preferred_element_type=f32) * scale
    scores = (scores * jnp.exp(log_inner - peak[..., None])).astype(bf16)
    from_block = jnp.einsum("hts,she->hte", scores, v, preferred_element_type=f32)
    from_state = jnp.einsum("thd,hde->hte", q, carried, preferred_element_type=f32)
    numerator = jnp.exp(log_inter - peak)[..., None] * from_state + from_block
    scaled = numerator * lax.rsqrt(
        jnp.mean(numerator * numerator, axis=-1, keepdims=True) + epsilon
    )
    gate = jax.nn.sigmoid(out_gate.astype(f32))
    return (scaled.transpose(1, 0, 2).reshape(length, heads * width) * gate).astype(bf16)


def slots_of(ids, first, capacity):
    rows, choices = ids.shape
    flat = ids.reshape(-1) - first
    onehot = (flat[:, None] == jnp.arange(GROUP)[None, :]).astype(bf16)
    count = rows * choices
    below = (jnp.arange(count)[:, None] > jnp.arange(count)[None, :]).astype(bf16)
    rank = jnp.sum(jnp.dot(below, onehot, preferred_element_type=f32) * onehot.astype(f32), axis=1)
    slot = flat * capacity + rank.astype(jnp.int32)
    inside = (flat >= 0) & (flat < GROUP)
    return jnp.where(inside, slot, -1).reshape(rows, choices)


def body(
    stream,
    queries,
    key_rows,
    value_rows,
    out_gate,
    in_gate,
    forget_gate,
    out_proj,
    ffn_gain,
    gate_proj,
    up_proj,
    down_proj,
    expert_ids,
    route_weights,
):
    total, mine = lax.axis_size("sp"), lax.axis_index("sp")
    groups = total // GROUP
    rows, width = stream.shape
    choices = expert_ids.shape[1]
    capacity = 2 * choices * rows // total
    cores = lax.axis_size("tp")

    def to_group(value, step):
        pairs = [
            (s, ((s // GROUP + step) % groups) * GROUP + s % GROUP) for s in range(total)
        ]
        return lax.ppermute(value, "sp", pairs)

    def other_core(value, step):
        return lax.ppermute(value, "tp", [(c, (c + step) % cores) for c in range(cores)])

    halves = [(gate_proj[0], up_proj[0], down_proj[0])] + [
        tuple(other_core(w[0], step) for w in (gate_proj, up_proj, down_proj))
        for step in range(1, cores)
    ]
    ids = [expert_ids] + [to_group(expert_ids, step) for step in range(1, groups)]
    shares = [route_weights] + [to_group(route_weights, step) for step in range(1, groups)]
    first = (mine // GROUP) * GROUP
    slot_count = GROUP * capacity
    places, backs = [], []
    for ids_one, share in zip(ids, shares):
        slot = slots_of(ids_one, first, capacity)
        hits = [
            (slot[:, j][None, :] == jnp.arange(slot_count)[:, None]) for j in range(choices)
        ]
        places.append(sum(hit.astype(bf16) for hit in hits))
        backs.append(sum(jnp.where(hits[j], share[:, j][None, :], 0.0) for j in range(choices)).astype(bf16))

    heads_out = mixer(queries, key_rows, value_rows, out_gate, in_gate, forget_gate)
    features = heads_out.shape[1]
    (token_heads,) = exchange(
        (heads_out.reshape(cores, rows, features),), ("slab",), "tp", cores, 3, 2_000_000
    )
    mix = sum(
        jnp.dot(token_heads[c], out_proj[c * features : (c + 1) * features], preferred_element_type=f32)
        for c in range(cores)
    )
    middle = (stream.astype(f32) + mix).astype(bf16)
    middle_float = middle.astype(f32)
    normed = (
        middle_float
        * lax.rsqrt(jnp.mean(middle_float * middle_float, axis=-1, keepdims=True) + epsilon)
        * ffn_gain
    ).astype(bf16)

    def experts(arrived):
        out = 0.0
        for gate, up, down in halves:
            hidden = (
                jax.nn.silu(jnp.dot(arrived, gate, preferred_element_type=f32))
                * jnp.dot(arrived, up, preferred_element_type=f32)
            ).astype(bf16)
            out = out + jnp.dot(hidden, down, preferred_element_type=f32)
        return out.astype(bf16)

    def round_trip(token_rows, place, back, turn):
        sent = jnp.dot(place, token_rows, preferred_element_type=f32).astype(bf16)
        cost = 40_000_000
        (arrived,) = exchange(
            (sent.reshape(GROUP, capacity, width),), ("slab",), "sp", GROUP, 4 + 2 * turn, cost
        )
        result = experts(arrived.reshape(slot_count, width)).reshape(GROUP, capacity, width)
        (returned,) = exchange((result,), ("slab",), "sp", GROUP, 5 + 2 * turn, cost)
        return lax.dot_general(
            back,
            returned.reshape(slot_count, width),
            (((0,), (0,)), ((), ())),
            preferred_element_type=f32,
        )

    crossing = [to_group(normed, step) for step in range(1, groups)]
    own = round_trip(normed, places[0], backs[0], 0)
    expert_sum = own
    for step in range(1, groups):
        done = round_trip(crossing[step - 1], places[step], backs[step], step).astype(bf16)
        expert_sum = expert_sum + to_group(done, groups - step).astype(f32)
    return (middle_float + expert_sum).astype(bf16)


def solution(mesh):
    in_specs = (
        P(("sp", "tp"), None),
        P("sp", "tp"),
        P("sp", "tp"),
        P("sp", "tp"),
        P("sp", "tp"),
        P("tp", "sp"),
        P("tp", "sp"),
        P(),
        P(),
        P("sp", None, "tp"),
        P("sp", None, "tp"),
        P("sp", "tp", None),
        P(("sp", "tp"), None),
        P(("sp", "tp"), None),
    )
    out_specs = P(("sp", "tp"), None)
    return jax.shard_map(body, mesh=mesh, in_specs=in_specs, out_specs=out_specs, check_vma=False)
```

time: 397 us -> 302 us (0.76)
  the two profiles are of different devices: /device:TPU:14 before, /device:TPU:6 now
where the time goes in v1:
time: 302 us; the launch traced here: 301 us
  Pallas kernels  207 us (69%)
  matrix products  64.2 us (21%)
  local copies, waits for them, and re-layouts  10 us (3%)
  other arithmetic  9.71 us (3%)
  starting transfers between devices  6.68 us (2%)
  waiting for transfers between devices  3.36 us (1%)
    pallas_call x7, Pallas kernels, exchange(): pl.pallas_call(functools.partial(exchange_kernel, axis, group, count, kin...  207 us
    dot_general x4, matrix products, experts(): out = out + jnp.dot(hidden, down, preferred_element_type=f32)  27.6 us
    dot_general x4, matrix products, experts(): jnp.dot(arrived, gate, preferred_element_type=f32)  15.7 us
    dot_general x2, matrix products, round_trip(): lax.dot_general(back, returned.reshape(slot_count, width), (((0,), (0,)),...  7.18 us
    ppermute x4, starting transfers between devices, to_group(): return lax.ppermute(value, 'sp', pairs)  6.1 us
  transfers between devices with their start and end apart: 7, of which 1 were waited for; matrix products, arithmetic and copies ran while one was open for 23% of the time, Pallas kernels for 57%

profile of v1, /device:TPU:6, one launch (start us, length us, event | category | flops | bytes accessed | tf_op | source)
XLA Modules:
  0.0 300.9 jit_solution(2897724488713030042)
XLA Ops:
  0.0 0.5 collective-permute-start.1
  0.7 0.7 fusion.84
  1.5 0.4 reduce_window_sum.22
  2.0 0.2 subtract_reduce_fusion
  2.3 0.2 slice_reduce_fusion.4
  2.5 1.3 copy.74
  3.8 1.1 copy.73
  4.9 0.9 fusion.106
  5.8 0.2 scatter.9.refs_1_
  6.0 1.0 convolution_convert_fusion.4
  7.0 12.4 %shard_map.136 = (bf16[16,16,256]{2,1,0:T(8,128)(2,1)}, f32[16,8,128]{2,1,0:T(8,128)}) custom-call(bf16[16,16,256]{2,1,0:T(8,128)(2,1)} %bitcast.136, f32[8,128]{1,0:T(8,128)} %copy-done.6), custom_call_target="tpu_custom_call" | custom-call | bytes 10000000 | tf_op jit(solution)/shard_map/pallas_call | solution.py:54
  19.4 0.9 fusion.107
  20.5 0.9 copy.76
  21.5 0.2 select_reduce_fusion
  21.7 0.3 convolution_convert_fusion
  22.1 0.7 copy.77
  22.7 10.2 %shard_map.137 = bf16[16,16,256]{2,1,0:T(8,128)(2,1)} custom-call(bf16[16,16,256]{2,1,0:T(8,128)(2,1)} %bitcast.139), custom_call_target="tpu_custom_call" | custom-call | bytes 10000000 | tf_op jit(solution)/shard_map/pallas_call | solution.py:54
  32.9 0.2 dynamic-slice_reduce_fusion
  33.1 1.2 fusion.53
  34.4 0.5 fusion.9
  35.0 2.1 fusion.18
  37.1 1.5 fusion.19
  38.6 0.3 copy.69
  39.0 1.1 multiply_convert_fusion.1
  40.0 3.5 %shard_map.138 = bf16[2,256,512]{2,1,0:T(8,128)(2,1)} custom-call(bf16[2,256,512]{2,1,0:T(8,128)(2,1)} %bitcast.133), custom_call_target="tpu_custom_call" | custom-call | bytes 2000000 | tf_op jit(solution)/shard_map/pallas_call | solution.py:54
  43.5 2.5 fusion.7
  46.1 0.3 copy-done.1
  46.4 1.9 fusion.2
  48.4 0.3 fusion.4
  48.7 2.1 collective-permute-start.5
  50.8 0.1 copy.70
  50.9 1.0 collective-permute-start.3
  51.9 0.7 broadcast_subtract_fusion.1
  52.5 1.0 sub.97
  53.6 0.3 fusion.15
  53.9 0.8 convert_element_type.126
  54.7 0.9 add_select_fusion.2
  55.6 0.2 slice_reduce_fusion.3
  55.8 2.1 convolution_convert_fusion.2
  57.9 59.1 %shard_map.139 = bf16[8,64,2048]{2,1,0:T(8,128)(2,1)} custom-call(bf16[8,64,2048]{2,1,0:T(8,128)(2,1)} %bitcast.118), custom_call_target="tpu_custom_call" | custom-call | bytes 40000000 | tf_op jit(solution)/shard_map/pallas_call | solution.py:54
  117.1 4.2 %fusion.95 = f32[512,384]{1,0:T(8,128)} fusion(bf16[512,2048]{1,0:T(8,128)(2,1)} %bitcast.122, bf16[1,2048,384]{2,1,0:T(8,128)(2,1)} %param.27), kind=kOutput, calls=%fused_computation.147 | convolution fusion | flops 805306368 | bytes 4456448 | tf_op jit(solution)/shard_map/dot_general | solution.py:214
  121.2 7.0 %fusion.14 = f32[512,2048]{1,0:T(8,128)} fusion(bf16[512,2048]{1,0:T(8,128)(2,1)} %bitcast.123, f32[512,384]{1,0:T(8,128)} %fusion.95, bf16[1,384,2048]{2,1,0:T(8,128)(2,1)} %param.29, bf16[1,2048,384]{2,1,0:T(8,128)(2,1)} %param.28), kind=kOutput, calls=%fused_computation.28 | convolution fusion | flops 1611792384 | bytes 10223616 | tf_op jit(solution)/shard_map/dot_general | solution.py:217
  128.3 0.2 collective-permute-start.4
  128.5 0.9 broadcast_subtract_fusion
  129.4 0.1 sub.99
  129.5 3.3 %collective-permute-done.4 = f32[256,2]{0,1:T(2,128)} collective-permute-done((f32[256,2]{0,1:T(2,128)S(1)}, f32[256,2]{0,1:T(2,128)}, u32[]{:S(2)}, u32[]{:S(2)}) %collective-permute-start.4) | collective-permute-done | bytes 2080 | tf_op jit(solution)/shard_map/ppermute | solution.py:171
  132.9 0.8 fusion.109
  133.6 0.3 fusion.16
  133.9 0.1 convert_element_type.138
  134.0 0.9 add_select_fusion.1
  135.0 0.2 slice_reduce_fusion.1
  135.2 2.1 convolution_convert_fusion.1
  137.2 32.5 %shard_map.141 = bf16[8,64,2048]{2,1,0:T(8,128)(2,1)} custom-call(bf16[8,64,2048]{2,1,0:T(8,128)(2,1)} %bitcast.117), custom_call_target="tpu_custom_call" | custom-call | bytes 40000000 | tf_op jit(solution)/shard_map/pallas_call | solution.py:54
  169.8 4.4 %fusion.93 = f32[512,384]{1,0:T(8,128)} fusion(bf16[512,2048]{1,0:T(8,128)(2,1)} %bitcast.126, bf16[1,2048,384]{2,1,0:T(8,128)(2,1)} %param.27), kind=kOutput, calls=%fused_computation.145 | convolution fusion | flops 805306368 | bytes 4456448 | tf_op jit(solution)/shard_map/dot_general | solution.py:214
  174.2 6.4 %fusion.13 = f32[512,2048]{1,0:T(8,128)} fusion(bf16[512,2048]{1,0:T(8,128)(2,1)S(1)} %bitcast.127, f32[512,384]{1,0:T(8,128)} %fusion.93, bf16[1,384,2048]{2,1,0:T(8,128)(2,1)} %param.29, bf16[1,2048,384]{2,1,0:T(8,128)(2,1)} %param.28), kind=kOutput, calls=%fused_computation.27 | convolution fusion | flops 1611792384 | bytes 10223616 | tf_op jit(solution)/shard_map/dot_general | solution.py:217
  180.7 3.5 %fusion.117 = f32[512,384]{1,0:T(8,128)} fusion(bf16[512,2048]{1,0:T(8,128)(2,1)S(1)} %bitcast.128, bf16[2048,384]{1,0:T(8,128)(2,1)} %collective-permute-done), kind=kOutput, calls=%fused_computation.165 | convolution fusion | flops 805306368 | bytes 4456448 | tf_op jit(solution)/shard_map/dot_general | solution.py:214
  184.2 7.0 %add_convert_fusion = bf16[512,2048]{1,0:T(8,128)(2,1)} fusion(f32[512,2048]{1,0:T(8,128)} %fusion.13, bf16[384,2048]{1,0:T(8,128)(2,1)} %collective-permute-done.2, f32[512,384]{1,0:T(8,128)} %fusion.117, bf16[512,2048]{1,0:T(8,128)(2,1)S(1)} %bitcast.129, bf16[2048,384]{1,0:T(8,128)(2,1)} %collective-permute-done.1), kind=kOutput, calls=%fused_computation.1 | convolution fusion | flops 1613889536 | bytes 12320768 | tf_op jit(solution)/shard_map/dot_general | solution.py:217
  191.2 35.3 %shard_map.142 = bf16[8,64,2048]{2,1,0:T(8,128)(2,1)} custom-call(bf16[8,64,2048]{2,1,0:T(8,128)(2,1)} %bitcast.132), custom_call_target="tpu_custom_call" | custom-call | bytes 40000000 | tf_op jit(solution)/shard_map/pallas_call | solution.py:54
  226.6 3.5 %convolution_convert_fusion.3 = bf16[256,2048]{1,0:T(8,128)(2,1)} fusion(bf16[512,2048]{1,0:T(8,128)(2,1)} %bitcast.116, f32[256]{0:T(256)S(1)} %bitcast.144, s32[256]{0:T(256)S(1)} %get-tuple-element.36, f32[256]{0:T(256)S(1)} %bitcast.143, s32[256]{0:T(256)S(1)} %get-tuple-element.35), kind=kOutput, calls=%fused_computation.11 | convolution fusion | flops 538181632 | bytes 3149824 | tf_op jit(solution)/shard_map/dot_general | solution.py:228
  230.1 2.9 collective-permute-start.6
  232.9 3.5 %fusion.116 = f32[512,384]{1,0:T(8,128)} fusion(bf16[512,2048]{1,0:T(8,128)(2,1)S(1)} %bitcast.124, bf16[2048,384]{1,0:T(8,128)(2,1)} %collective-permute-done), kind=kOutput, calls=%fused_computation.164 | convolution fusion | flops 805306368 | bytes 4456448 | tf_op jit(solution)/shard_map/dot_general | solution.py:214
  236.4 7.1 %add_convert_fusion.1 = bf16[512,2048]{1,0:T(8,128)(2,1)} fusion(f32[512,2048]{1,0:T(8,128)} %fusion.14, bf16[384,2048]{1,0:T(8,128)(2,1)} %collective-permute-done.2, f32[512,384]{1,0:T(8,128)} %fusion.116, bf16[512,2048]{1,0:T(8,128)(2,1)S(1)} %bitcast.125, bf16[2048,384]{1,0:T(8,128)(2,1)} %collective-permute-done.1), kind=kOutput, calls=%fused_computation.2 | convolution fusion | flops 1613889536 | bytes 12320768 | tf_op jit(solution)/shard_map/dot_general | solution.py:217
  243.5 53.6 %shard_map.140 = bf16[8,64,2048]{2,1,0:T(8,128)(2,1)} custom-call(bf16[8,64,2048]{2,1,0:T(8,128)(2,1)} %bitcast.131), custom_call_target="tpu_custom_call" | custom-call | bytes 40000000 | tf_op jit(solution)/shard_map/pallas_call | solution.py:54
  297.2 3.7 %fusion.5 = bf16[256,2048]{1,0:T(8,128)(2,1)} fusion(bf16[256,2048]{1,0:T(8,128)(2,1)S(1)} %get-tuple-element.54, bf16[256,2048]{1,0:T(8,128)(2,1)} %collective-permute-done.6, bf16[512,2048]{1,0:T(8,128)(2,1)} %bitcast.130, f32[256]{0:T(256)S(1)} %bitcast.151, s32[256]{0:T(256)S(1)} %copy-done.11, f32[256]{0:T(256)S(1)} %bitcast.150, s32[256]{0:T(256)S(1)} %copy-done.9), kind=kOutput, calls=%fused_computation.15 | convolution fusion | flops 540278784 | bytes 5246976 | tf_op jit(solution)/shard_map/dot_general | solution.py:228
  (58 shorter events, 1.1 us)
Async XLA Ops:
  0.0 33.1 %copy-start = (bf16[512,256]{1,0:T(8,128)(2,1)S(1)}, bf16[512,256]{1,0:T(8,128)(2,1)}, u32[]{:S(2)}) copy-start(bf16[512,256]{1,0:T(8,128)(2,1)} %param.19) | copy-start | bytes 786436
  0.0 180.7 %collective-permute-start = (bf16[2048,384]{1,0:T(8,128)(2,1)}, bf16[2048,384]{1,0:T(8,128)(2,1)}, u32[]{:S(2)}, u32[]{:S(2)}) collective-permute-start(bf16[2048,384]{1,0:T(8,128)(2,1)} %bitcast.152), channel_id=1, source_target_pairs={{0,1},{1,0},{2,3},{3,2},{4,5},{5,4},{6,7},{7,6},{8,9},{9,8},{10,11... | collective-permute-start | bytes 4718600 | tf_op jit(solution)/shard_map/ppermute | solution.py:174
  0.0 184.2 %collective-permute-start.1 = (bf16[2048,384]{1,0:T(8,128)(2,1)}, bf16[2048,384]{1,0:T(8,128)(2,1)}, u32[]{:S(2)}, u32[]{:S(2)}) collective-permute-start(bf16[2048,384]{1,0:T(8,128)(2,1)} %bitcast.153), channel_id=1, source_target_pairs={{0,1},{1,0},{2,3},{3,2},{4,5},{5,4},{6,7},{7,6},{8,9},{9,8},{10,11... | collective-permute-start | bytes 4718600 | tf_op jit(solution)/shard_map/ppermute | solution.py:174
  0.5 183.7 %collective-permute-start.2 = (bf16[384,2048]{1,0:T(8,128)(2,1)}, bf16[384,2048]{1,0:T(8,128)(2,1)}, u32[]{:S(2)}, u32[]{:S(2)}) collective-permute-start(bf16[384,2048]{1,0:T(8,128)(2,1)} %bitcast.154), channel_id=1, source_target_pairs={{0,1},{1,0},{2,3},{3,2},{4,5},{5,4},{6,7},{7,6},{8,9},{9,8},{10,11... | collective-permute-start | bytes 4718600 | tf_op jit(solution)/shard_map/ppermute | solution.py:174
  6.0 1.0 copy-start.6
  37.1 1.9 copy-start.5
  40.0 6.0 %copy-start.4 = (bf16[256,2048]{1,0:T(8,128)(2,1)S(1)}, bf16[256,2048]{1,0:T(8,128)(2,1)}, u32[]{:S(2)}) copy-start(bf16[256,2048]{1,0:T(8,128)(2,1)} %param.18) | copy-start | bytes 3145732
  43.5 2.9 copy-start.1
  46.4 1.9 copy-start.7
  48.3 2.4 copy-start.12
  48.7 86.5 %collective-permute-start.5 = (bf16[256,2048]{1,0:T(8,128)(2,1)S(1)}, bf16[256,2048]{1,0:T(8,128)(2,1)S(1)}, u32[]{:S(2)}, u32[]{:S(2)}) collective-permute-start(bf16[256,2048]{1,0:T(8,128)(2,1)S(1)} %fusion.4), channel_id=1, source_target_pairs={{0,16},{2,18},{4,20},{6,22},{8,24},{10,26},{12,28},{14,30},{16,0},... | collective-permute-start | bytes 3145736 | tf_op jit(solution)/shard_map/ppermute | solution.py:171
  50.9 77.4 %collective-permute-start.3 = (s32[256,2]{1,0:T(8,128)S(1)}, s32[256,2]{1,0:T(8,128)}, u32[]{:S(2)}, u32[]{:S(2)}) collective-permute-start(s32[256,2]{1,0:T(8,128)S(1)} %copy.70), channel_id=1, source_target_pairs={{0,16},{2,18},{4,20},{6,22},{8,24},{10,26},{12,28},{14,30},{16,0},... | collective-permute-start | bytes 6152 | tf_op jit(solution)/shard_map/ppermute | solution.py:171
  55.8 2.1 copy-start.8
  55.8 2.1 copy-start.10
  121.2 7.0 %copy-start.13 = (f32[256,2]{0,1:T(2,128)S(1)}, f32[256,2]{0,1:T(2,128)}, u32[]{:S(2)}) copy-start(f32[256,2]{0,1:T(2,128)} %param.31) | copy-start | bytes 6148
  128.3 4.6 %collective-permute-start.4 = (f32[256,2]{0,1:T(2,128)S(1)}, f32[256,2]{0,1:T(2,128)}, u32[]{:S(2)}, u32[]{:S(2)}) collective-permute-start(f32[256,2]{0,1:T(2,128)S(1)} %copy-done.13), channel_id=1, source_target_pairs={{0,16},{2,18},{4,20},{6,22},{8,24},{10,26},{12,28},{14,30},{16,0},... | collective-permute-start | bytes 6152 | tf_op jit(solution)/shard_map/ppermute | solution.py:171
  169.8 4.5 %copy-start.3 = (bf16[8,64,2048]{2,1,0:T(8,128)(2,1)S(1)}, bf16[8,64,2048]{2,1,0:T(8,128)(2,1)}, u32[]{:S(2)}) copy-start(bf16[8,64,2048]{2,1,0:T(8,128)(2,1)} %shard_map.141) | copy-start | bytes 6291460
  226.6 6.4 %copy-start.14 = (f32[256,2]{0,1:T(2,128)S(1)}, f32[256,2]{0,1:T(2,128)}, u32[]{:S(2)}) copy-start(f32[256,2]{0,1:T(2,128)} %param.31) | copy-start | bytes 6148
  226.6 6.3 %copy-start.2 = (bf16[8,64,2048]{2,1,0:T(8,128)(2,1)S(1)}, bf16[8,64,2048]{2,1,0:T(8,128)(2,1)}, u32[]{:S(2)}) copy-start(bf16[8,64,2048]{2,1,0:T(8,128)(2,1)} %shard_map.139) | copy-start | bytes 6291460
  230.1 67.1 %collective-permute-start.6 = (bf16[256,2048]{1,0:T(8,128)(2,1)}, bf16[256,2048]{1,0:T(8,128)(2,1)}, u32[]{:S(2)}, u32[]{:S(2)}) collective-permute-start(bf16[256,2048]{1,0:T(8,128)(2,1)} %convolution_convert_fusion.3), channel_id=1, source_target_pairs={{0,16},{2,18},{4,20},{6,22},{8,24},{10,26},{12,28},{14,30},{16,0},... | collective-permute-start | bytes 3145736 | tf_op jit(solution)/shard_map/ppermute | solution.py:171
  243.5 53.7 %copy-start.9 = (s32[256]{0:T(256)S(1)}, s32[256]{0:T(256)}, u32[]{:S(2)}) copy-start(s32[256]{0:T(256)} %copy-done.8) | copy-start | bytes 3076
  243.5 53.7 %copy-start.11 = (s32[256]{0:T(256)S(1)}, s32[256]{0:T(256)}, u32[]{:S(2)}) copy-start(s32[256]{0:T(256)} %copy-done.10) | copy-start | bytes 3076

commit v2 on v1

--- a/solution.py
+++ b/solution.py
@@ -141,6 +141,265 @@
     return jnp.where(inside, slot, -1).reshape(rows, choices)
 
 
+CHUNKS = 2
+TILE = 256
+FLIPS = (7, 3, 5, 6, 1, 2, 4)
+
+
+def flip(member, bits):
+    for power in (1, 2, 4):
+        if bits & power:
+            member = member + power * (1 - 2 * (lax.rem(lax.div(member, power), 2)))
+    return member
+
+
+def expert_kernel(groups, capacity, halves, *refs):
+    normed, middle, places, backs = refs[:4]
+    weights_hbm = refs[4 : 4 + 3 * halves]
+    out = refs[4 + 3 * halves]
+    rest = refs[5 + 3 * halves :]
+    weights = rest[: 3 * halves]
+    crossed, combined, crossed_back, own_sum, hidden = rest[3 * halves : 3 * halves + 5]
+    sent0, arrived0, result0, back0, sent1, arrived1, result1, back1 = rest[
+        3 * halves + 5 : 3 * halves + 13
+    ]
+    load_sem, cross_s, cross_r, home_s, home_r, own_s, own_r, oth_s, oth_r = rest[3 * halves + 13 :]
+    rows, width = normed.shape
+    part = width // CHUNKS
+    extra = groups - 1
+    mine = lax.axis_index("sp")
+    group = lax.div(mine, GROUP)
+    base = group * GROUP
+    me = mine - base
+    far = lambda step: lax.rem(group + step, groups) * GROUP + me
+
+    loads = [
+        pltpu.make_async_copy(src, dst, load_sem.at[n])
+        for n, (src, dst) in enumerate(zip(weights_hbm, weights))
+    ]
+    for load in loads:
+        load.start()
+    barrier = pltpu.get_barrier_semaphore()
+    peers = [base + flip(me, bits) for bits in FLIPS] + [far(step) for step in range(1, groups)]
+    for peer in peers:
+        pl.semaphore_signal(
+            barrier, inc=1, device_id={"sp": peer}, device_id_type=pl.DeviceIdType.MESH
+        )
+    pl.semaphore_wait(barrier, len(peers))
+
+    def send(src, dst, send_sem, recv_sem, peer):
+        copy = pltpu.make_async_remote_copy(
+            src_ref=src,
+            dst_ref=dst,
+            send_sem=send_sem,
+            recv_sem=recv_sem,
+            device_id={"sp": peer},
+            device_id_type=pl.DeviceIdType.MESH,
+        )
+        copy.start()
+        return copy
+
+    def box_send(src, dst, send_sem, recv_sem, cols):
+        copies = []
+        for n, bits in enumerate(FLIPS):
+            to = flip(me, bits)
+            copies.append(
+                send(
+                    src.at[to, :, cols],
+                    dst.at[me, :, cols],
+                    send_sem.at[n],
+                    recv_sem.at[n],
+                    base + to,
+                )
+            )
+        return copies
+
+    def tiles(start, stop, body):
+        def turn(n, carry):
+            body(pl.ds(pl.multiple_of(start + n * TILE, TILE), TILE))
+            return carry
+
+        lax.fori_loop(0, (stop - start) // TILE, turn, 0)
+
+    def columns(chunk):
+        return pl.ds(chunk * part, part)
+
+    crossing = [
+        [
+            send(
+                normed.at[:, columns(chunk)],
+                crossed.at[step - 1, :, columns(chunk)],
+                cross_s.at[step - 1, chunk],
+                cross_r.at[step - 1, chunk],
+                far(step),
+            )
+            for step in range(1, groups)
+        ]
+        for chunk in range(CHUNKS)
+    ]
+
+    def place_own(cols):
+        value = jnp.dot(places[0], normed[:, cols], preferred_element_type=f32)
+        sent0[:, :, cols] = value.astype(bf16).reshape(GROUP, capacity, TILE)
+
+    tiles(0, width, place_own)
+    own = box_send(sent0, arrived0, own_s.at[0], own_r.at[0], pl.ds(0, width))
+    arrived0[me] = sent0[me]
+
+    others = []
+    for chunk in range(CHUNKS):
+        for copy in crossing[chunk]:
+            copy.wait()
+
+        def place_other(cols):
+            for step in range(extra):
+                value = jnp.dot(
+                    places[step + 1], crossed[step, :, cols], preferred_element_type=f32
+                )
+                sent1[:, step * capacity : (step + 1) * capacity, cols] = value.astype(
+                    bf16
+                ).reshape(GROUP, capacity, TILE)
+
+        tiles(chunk * part, (chunk + 1) * part, place_other)
+        others += box_send(sent1, arrived1, oth_s.at[chunk], oth_r.at[chunk], columns(chunk))
+    arrived1[me] = sent1[me]
+
+    def make_hidden(arrived, amount):
+        wide = GROUP * amount
+        members = max(1, min(GROUP, TILE // amount))
+        high = members * amount
+
+        def turn(n, carry):
+            value = arrived[pl.ds(n * members, members)].reshape(high, width)
+            for half in range(halves):
+                gate = jnp.dot(value, weights[3 * half][...], preferred_element_type=f32)
+                up = jnp.dot(value, weights[3 * half + 1][...], preferred_element_type=f32)
+                units = gate.shape[1]
+                hidden[pl.ds(pl.multiple_of(n * high, 16), high), half * units : (half + 1) * units] = (
+                    gate * jax.nn.sigmoid(gate) * up
+                ).astype(bf16)
+            return carry
+
+        lax.fori_loop(0, wide // high, turn, 0)
+
+    def make_result(result, amount, chunk, parts):
+        wide = GROUP * amount
+        units = weights[2].shape[0]
+        step = width // parts
+
+        def one(cols):
+            value = sum(
+                jnp.dot(
+                    hidden[:wide, half * units : (half + 1) * units],
+                    weights[3 * half + 2][:, cols],
+                    preferred_element_type=f32,
+                )
+                for half in range(halves)
+            )
+            result[:, :, cols] = value.astype(bf16).reshape(GROUP, amount, TILE)
+
+        tiles(chunk * step, (chunk + 1) * step, one)
+
+    for load in loads:
+        load.wait()
+    for copy in own:
+        copy.wait()
+    make_hidden(arrived0, capacity)
+    make_result(result0, capacity, 0, 1)
+
+    for copy in others:
+        copy.wait()
+    returns = []
+    if extra:
+        make_hidden(arrived1, extra * capacity)
+        for chunk in range(CHUNKS):
+            make_result(result1, extra * capacity, chunk, CHUNKS)
+            at = CHUNKS + chunk
+            returns.append(box_send(result1, back1, oth_s.at[at], oth_r.at[at], columns(chunk)))
+        back1[me] = result1[me]
+    own_return = box_send(result0, back0, own_s.at[1], own_r.at[1], pl.ds(0, width))
+    back0[me] = result0[me]
+
+    homeward = []
+    for chunk in range(CHUNKS):
+        for copy in returns[chunk]:
+            copy.wait()
+
+        def combine(cols):
+            for step in range(extra):
+                value = back1[:, step * capacity : (step + 1) * capacity, cols]
+                combined[step, :, cols] = jnp.dot(
+                    backs[step + 1],
+                    value.reshape(GROUP * capacity, TILE),
+                    preferred_element_type=f32,
+                ).astype(bf16)
+
+        tiles(chunk * part, (chunk + 1) * part, combine)
+        homeward.append(
+            [
+                send(
+                    combined.at[step, :, columns(chunk)],
+                    crossed_back.at[step, :, columns(chunk)],
+                    home_s.at[step, chunk],
+                    home_r.at[step, chunk],
+                    far(groups - 1 - step),
+                )
+                for step in range(extra)
+            ]
+        )
+
+    for copy in own_return:
+        copy.wait()
+
+    def combine_own(cols):
+        own_sum[:, cols] = middle[:, cols].astype(f32) + jnp.dot(
+            backs[0],
+            back0[:, :, cols].reshape(GROUP * capacity, TILE),
+            preferred_element_type=f32,
+        )
+
+    tiles(0, width, combine_own)
+    for chunk in range(CHUNKS):
+        for copy in homeward[chunk]:
+            copy.wait()
+        cols = slice(chunk * part, (chunk + 1) * part)
+        total = own_sum[:, cols]
+        for step in range(extra):
+            total = total + crossed_back[step, :, cols].astype(f32)
+        out[:, cols] = total.astype(bf16)
+
+
+def expert_layer(arrays, weights, groups, capacity):
+    rows, width = arrays[0].shape
+    extra = groups - 1
+    halves = len(weights) // 3
+    units = sum(weights[3 * half].shape[1] for half in range(halves))
+    own = pltpu.VMEM((GROUP, capacity, width), bf16)
+    other = pltpu.VMEM((GROUP, extra * capacity, width), bf16)
+    cross = pltpu.VMEM((extra, rows, width), bf16)
+    dma = pltpu.SemaphoreType.DMA
+    scratch = [pltpu.VMEM(w.shape, w.dtype) for w in weights]
+    scratch += [cross, cross, cross, pltpu.VMEM((rows, width), f32)]
+    scratch += [pltpu.VMEM((GROUP * max(1, extra) * capacity, units), bf16)]
+    scratch += [own] * 4 + [other] * 4
+    scratch += [dma((len(weights),))] + [dma((extra, CHUNKS))] * 4
+    scratch += [dma((2, len(FLIPS)))] * 2 + [dma((2 * CHUNKS, len(FLIPS)))] * 2
+    vmem, anywhere = pl.BlockSpec(memory_space=pltpu.VMEM), pl.BlockSpec(memory_space=pl.ANY)
+    return pl.pallas_call(
+        functools.partial(expert_kernel, groups, capacity, halves),
+        out_shape=jax.ShapeDtypeStruct((rows, width), bf16),
+        in_specs=[vmem] * 4 + [anywhere] * len(weights),
+        out_specs=vmem,
+        scratch_shapes=scratch,
+        compiler_params=pltpu.CompilerParams(
+            collective_id=4, has_side_effects=True, vmem_limit_bytes=64 * 1024 * 1024 - 65536
+        ),
+        cost_estimate=pl.CostEstimate(
+            flops=10_000_000_000, bytes_accessed=100_000_000, transcendentals=0
+        ),
+    )(*arrays, *weights)
+
+
 def body(
     stream,
     queries,
@@ -184,11 +443,16 @@
     places, backs = [], []
     for ids_one, share in zip(ids, shares):
         slot = slots_of(ids_one, first, capacity)
-        hits = [
-            (slot[:, j][None, :] == jnp.arange(slot_count)[:, None]) for j in range(choices)
-        ]
-        places.append(sum(hit.astype(bf16) for hit in hits))
-        backs.append(sum(jnp.where(hits[j], share[:, j][None, :], 0.0) for j in range(choices)).astype(bf16))
+        here = jnp.arange(slot_count)
+        places.append(
+            sum((slot[:, j][None, :] == here[:, None]).astype(bf16) for j in range(choices))
+        )
+        backs.append(
+            sum(
+                jnp.where(slot[:, j][:, None] == here[None, :], share[:, j][:, None], 0.0)
+                for j in range(choices)
+            ).astype(bf16)
+        )
 
     heads_out = mixer(queries, key_rows, value_rows, out_gate, in_gate, forget_gate)
     features = heads_out.shape[1]
@@ -207,38 +471,8 @@
         * ffn_gain
     ).astype(bf16)
 
-    def experts(arrived):
-        out = 0.0
-        for gate, up, down in halves:
-            hidden = (
-                jax.nn.silu(jnp.dot(arrived, gate, preferred_element_type=f32))
-                * jnp.dot(arrived, up, preferred_element_type=f32)
-            ).astype(bf16)
-            out = out + jnp.dot(hidden, down, preferred_element_type=f32)
-        return out.astype(bf16)
-
-    def round_trip(token_rows, place, back, turn):
-        sent = jnp.dot(place, token_rows, preferred_element_type=f32).astype(bf16)
-        cost = 40_000_000
-        (arrived,) = exchange(
-            (sent.reshape(GROUP, capacity, width),), ("slab",), "sp", GROUP, 4 + 2 * turn, cost
-        )
-        result = experts(arrived.reshape(slot_count, width)).reshape(GROUP, capacity, width)
-        (returned,) = exchange((result,), ("slab",), "sp", GROUP, 5 + 2 * turn, cost)
-        return lax.dot_general(
-            back,
-            returned.reshape(slot_count, width),
-            (((0,), (0,)), ((), ())),
-            preferred_element_type=f32,
-        )
-
-    crossing = [to_group(normed, step) for step in range(1, groups)]
-    own = round_trip(normed, places[0], backs[0], 0)
-    expert_sum = own
-    for step in range(1, groups):
-        done = round_trip(crossing[step - 1], places[step], backs[step], step).astype(bf16)
-        expert_sum = expert_sum + to_group(done, groups - step).astype(f32)
-    return (middle_float + expert_sum).astype(bf16)
+    arrays = (normed, middle, jnp.stack(places), jnp.stack(backs))
+    return expert_layer(arrays, [w for half in halves for w in half], groups, capacity)
 
 
 def solution(mesh):

time: 302 us -> 226 us (0.75)
  the two profiles are of different devices: /device:TPU:6 before, /device:TPU:0 now
where the time goes in v2:
time: 226 us; the launch traced here: 225 us
  Pallas kernels  191 us (85%)
  local copies, waits for them, and re-layouts  12.1 us (5%)
  matrix products  9.58 us (4%)
  other arithmetic  7.69 us (3%)
  starting transfers between devices  4.72 us (2%)
    pallas_call x1, Pallas kernels, expert_layer(): pl.pallas_call(functools.partial(expert_kernel, groups, capacity, halves)...  165 us
    pallas_call x3, Pallas kernels, exchange(): pl.pallas_call(functools.partial(exchange_kernel, axis, group, count, kin...  26.1 us
    unnamed x20, local copies, waits for them, and re-layouts  5.83 us
  transfers between devices with their start and end apart: 5, of which 0 were waited for; matrix products, arithmetic and copies ran while one was open for 11% of the time, Pallas kernels for 12%

profile of v2, /device:TPU:0, one launch (start us, length us, event | category | flops | bytes accessed | tf_op | source)
XLA Modules:
  0.0 225.3 jit_solution(14079179493889875696)
XLA Ops:
  0.0 0.8 copy.70
  0.8 4.1 %collective-permute-start = (s32[256,2]{1,0:T(8,128)S(1)}, s32[256,2]{1,0:T(8,128)S(1)}, u32[]{:S(2)}, u32[]{:S(2)}) collective-permute-start(s32[256,2]{1,0:T(8,128)S(1)} %copy.70), channel_id=1, source_target_pairs={{0,16},{2,18},{4,20},{6,22},{8,24},{10,26},{12,28},{14,30},{16,0},... | collective-permute-start | bytes 6152 | tf_op jit(solution)/shard_map/ppermute | solution.py:430
  5.0 0.1 collective-permute-start.1
  5.0 0.5 collective-permute-start.3
  5.6 0.0 collective-permute-start.4
  5.6 0.1 iota_compare_fusion.3
  5.7 0.0 copy-start.4
  5.7 0.8 fusion.54
  6.5 0.7 fusion.46
  7.2 0.1 reshape.693
  7.2 0.4 reduce_window_sum.22
  7.7 0.1 slice.103
  7.8 0.2 subtract_reduce_fusion
  7.9 0.1 broadcast_add_fusion
  8.0 0.1 add.175
  8.1 0.2 slice_reduce_fusion.4
  8.3 1.3 copy.74
  9.5 1.1 copy.73
  10.7 0.2 fusion.52
  10.8 0.1 multiply_bitcast_fusion
  10.9 0.2 scatter.9.refs_1_
  11.1 1.0 convolution_convert_fusion.1
  12.1 11.8 %shard_map.136 = (bf16[16,16,256]{2,1,0:T(8,128)(2,1)}, f32[16,8,128]{2,1,0:T(8,128)}) custom-call(bf16[16,16,256]{2,1,0:T(8,128)(2,1)} %bitcast.82, f32[8,128]{1,0:T(8,128)} %copy-done.5), custom_call_target="tpu_custom_call" | custom-call | bytes 10000000 | tf_op jit(solution)/shard_map/pallas_call | solution.py:54
  23.9 0.9 fusion.53
  24.8 0.1 copy.62
  24.9 0.1 copy.63
  25.0 0.9 copy.76
  26.0 0.2 select_reduce_fusion
  26.1 0.1 fusion.51
  26.2 0.3 convolution_convert_fusion
  26.6 0.7 copy.77
  27.3 10.8 %shard_map.137 = bf16[16,16,256]{2,1,0:T(8,128)(2,1)} custom-call(bf16[16,16,256]{2,1,0:T(8,128)(2,1)} %bitcast.85), custom_call_target="tpu_custom_call" | custom-call | bytes 10000000 | tf_op jit(solution)/shard_map/pallas_call | solution.py:54
  38.1 0.2 dynamic-slice_reduce_fusion
  38.2 1.2 fusion.29
  39.5 0.5 fusion.8
  40.0 0.1 subtract_exponential_fusion
  40.1 2.1 fusion.13
  42.2 0.2 fusion.14
  42.4 0.0 copy-start.3
  42.5 0.3 copy.69
  42.8 0.7 copy-done.3
  43.5 1.1 multiply_convert_fusion.1
  44.6 3.5 %shard_map.138 = bf16[2,256,512]{2,1,0:T(8,128)(2,1)} custom-call(bf16[2,256,512]{2,1,0:T(8,128)(2,1)} %bitcast.79), custom_call_target="tpu_custom_call" | custom-call | bytes 2000000 | tf_op jit(solution)/shard_map/pallas_call | solution.py:54
  48.1 0.0 copy-start
  48.1 2.5 %fusion.6 = f32[256,2048]{1,0:T(8,128)S(1)} fusion(bf16[1024,2048]{1,0:T(8,128)(2,1)} %param.25, bf16[2,256,512]{2,1,0:T(8,128)(2,1)} %shard_map.138), kind=kOutput, calls=%fused_computation.10 | convolution fusion | flops 536870912 | bytes 4456448 | tf_op jit(solution)/shard_map/dot_general | solution.py:463
  50.6 0.3 copy-done
  51.0 1.9 fusion.2
  52.9 0.1 sub.97
  53.1 0.3 fusion.10
  53.4 0.1 convert_element_type.136
  53.6 1.3 fusion.4.refs_0_
  54.8 0.2 slice_reduce_fusion.3
  55.0 0.0 collective-permute-done
  55.1 0.1 sub.99
  55.2 0.3 fusion.11
  55.5 0.1 convert_element_type.142
  55.7 0.2 slice_reduce_fusion.1
  55.9 0.0 collective-permute-done.1
  55.9 0.3 add_convert_fusion
  56.3 0.8 pad_maximum_fusion.1.refs_3_
  57.1 0.3 fusion.25
  57.4 0.9 pad_maximum_fusion.refs_2_
  58.3 164.7 %shard_map.139 = bf16[256,2048]{1,0:T(8,128)(2,1)} custom-call(bf16[256,2048]{1,0:T(8,128)(2,1)} %fusion.4.refs_0_, bf16[256,2048]{1,0:T(8,128)(2,1)} %copy-done.1, bf16[2,512,256]{2,1,0:T(8,128)(2,1)} %pad_maximum_fusion.refs_2_, bf16[2,256,512]{2,1,0:T(8,128)(2,1)} %pad_maximum_fusion.1.refs_3_, bf16[2048,384]{1,0:T(8,128)(2,1)} %bitcast.99, ...), custom_call_target="tpu_custom_call" | custom-call | flops 10000000000 | bytes 100000000 | tf_op jit(solution)/shard_map/pallas_call | solution.py:388
  223.0 2.3 %copy.91 = bf16[256,2048]{1,0:T(8,128)(2,1)} copy(bf16[256,2048]{1,0:T(8,128)(2,1)} %shard_map.139) | data formatting | bytes 2097152
  (30 shorter events, 0.2 us)
Async XLA Ops:
  0.0 10.6 %copy-start.7 = (f32[2,512]{1,0:T(2,128)S(1)}, f32[2,512]{1,0:T(2,128)}, u32[]{:S(2)}) copy-start(f32[2,512]{1,0:T(2,128)} %param.23) | copy-start | bytes 12292
  0.8 54.2 %collective-permute-start = (s32[256,2]{1,0:T(8,128)S(1)}, s32[256,2]{1,0:T(8,128)S(1)}, u32[]{:S(2)}, u32[]{:S(2)}) collective-permute-start(s32[256,2]{1,0:T(8,128)S(1)} %copy.70), channel_id=1, source_target_pairs={{0,16},{2,18},{4,20},{6,22},{8,24},{10,26},{12,28},{14,30},{16,0},... | collective-permute-start | bytes 6152 | tf_op jit(solution)/shard_map/ppermute | solution.py:430
  5.0 50.9 %collective-permute-start.1 = (f32[256,2]{0,1:T(2,128)}, f32[256,2]{0,1:T(2,128)S(1)}, u32[]{:S(2)}, u32[]{:S(2)}) collective-permute-start(f32[256,2]{0,1:T(2,128)} %param.31), channel_id=1, source_target_pairs={{0,16},{2,18},{4,20},{6,22},{8,24},{10,26},{12,28},{14,30},{16,0},... | collective-permute-start | bytes 6152 | tf_op jit(solution)/shard_map/ppermute | solution.py:430
  5.0 53.2 %collective-permute-start.2 = (bf16[2048,384]{1,0:T(8,128)(2,1)}, bf16[2048,384]{1,0:T(8,128)(2,1)}, u32[]{:S(2)}, u32[]{:S(2)}) collective-permute-start(bf16[2048,384]{1,0:T(8,128)(2,1)} %bitcast.98), channel_id=1, source_target_pairs={{0,1},{1,0},{2,3},{3,2},{4,5},{5,4},{6,7},{7,6},{8,9},{9,8},{10,11... | collective-permute-start | bytes 4718600 | tf_op jit(solution)/shard_map/ppermute | solution.py:433
  5.0 53.2 %collective-permute-start.3 = (bf16[2048,384]{1,0:T(8,128)(2,1)}, bf16[2048,384]{1,0:T(8,128)(2,1)}, u32[]{:S(2)}, u32[]{:S(2)}) collective-permute-start(bf16[2048,384]{1,0:T(8,128)(2,1)} %bitcast.100), channel_id=1, source_target_pairs={{0,1},{1,0},{2,3},{3,2},{4,5},{5,4},{6,7},{7,6},{8,9},{9,8},{10,11... | collective-permute-start | bytes 4718600 | tf_op jit(solution)/shard_map/ppermute | solution.py:433
  5.6 52.7 %collective-permute-start.4 = (bf16[384,2048]{1,0:T(8,128)(2,1)}, bf16[384,2048]{1,0:T(8,128)(2,1)}, u32[]{:S(2)}, u32[]{:S(2)}) collective-permute-start(bf16[384,2048]{1,0:T(8,128)(2,1)} %bitcast.102), channel_id=1, source_target_pairs={{0,1},{1,0},{2,3},{3,2},{4,5},{5,4},{6,7},{7,6},{8,9},{9,8},{10,11... | collective-permute-start | bytes 4718600 | tf_op jit(solution)/shard_map/ppermute | solution.py:433
  5.7 32.6 %copy-start.4 = (bf16[512,256]{1,0:T(8,128)(2,1)S(1)}, bf16[512,256]{1,0:T(8,128)(2,1)}, u32[]{:S(2)}) copy-start(bf16[512,256]{1,0:T(8,128)(2,1)} %param.19) | copy-start | bytes 786436
  11.1 1.0 copy-start.5
  42.4 1.0 copy-start.3
  44.6 6.1 %copy-start.2 = (bf16[256,2048]{1,0:T(8,128)(2,1)S(1)}, bf16[256,2048]{1,0:T(8,128)(2,1)}, u32[]{:S(2)}) copy-start(bf16[256,2048]{1,0:T(8,128)(2,1)} %param.18) | copy-start | bytes 3145732
  48.1 2.9 %copy-start = (bf16[1024,2048]{1,0:T(8,128)(2,1)S(1)}, bf16[1024,2048]{1,0:T(8,128)(2,1)}, u32[]{:S(2)}) copy-start(bf16[1024,2048]{1,0:T(8,128)(2,1)} %param.25) | copy-start | bytes 12582916
  51.0 2.6 %copy-start.6 = (f32[2048]{0:T(1024)S(1)}, f32[2048]{0:T(1024)}, u32[]{:S(2)}) copy-start(f32[2048]{0:T(1024)} %param.26) | copy-start | bytes 24580
  52.9 2.6 %copy-start.1 = (bf16[256,2048]{1,0:T(8,128)(2,1)}, bf16[256,2048]{1,0:T(8,128)(2,1)S(1)}, u32[]{:S(2)}) copy-start(bf16[256,2048]{1,0:T(8,128)(2,1)S(1)} %get-tuple-element.54.refs_1_) | copy-start | bytes 3145732

commit v3 on v2

--- a/solution.py
+++ b/solution.py
@@ -141,9 +141,10 @@
     return jnp.where(inside, slot, -1).reshape(rows, choices)
 
 
-CHUNKS = 2
+CHUNKS = 4
 TILE = 256
 FLIPS = (7, 3, 5, 6, 1, 2, 4)
+ACROSS = 4
 
 
 def flip(member, bits):
@@ -171,7 +172,7 @@
     group = lax.div(mine, GROUP)
     base = group * GROUP
     me = mine - base
-    far = lambda step: lax.rem(group + step, groups) * GROUP + me
+    far = lambda step: lax.rem(group + step, groups) * GROUP + flip(me, ACROSS)
 
     loads = [
         pltpu.make_async_copy(src, dst, load_sem.at[n])
@@ -425,7 +426,7 @@
 
     def to_group(value, step):
         pairs = [
-            (s, ((s // GROUP + step) % groups) * GROUP + s % GROUP) for s in range(total)
+            (s, ((s // GROUP + step) % groups) * GROUP + (s % GROUP ^ ACROSS)) for s in range(total)
         ]
         return lax.ppermute(value, "sp", pairs)
 

time: 226 us -> 220 us (0.973)
  Pallas kernels: 191 us -> 184 us
    pallas_call x1, Pallas kernels: 165 us -> 158 us  [expert_layer(): pl.pallas_call(functools.partial(expert_kernel, groups, capacity, halves)...]
where the time goes in v3:
time: 220 us
  Pallas kernels  184 us (84%)
  local copies, waits for them, and re-layouts  12.1 us (6%)
  matrix products  9.58 us (4%)
  other arithmetic  7.69 us (3%)
  starting transfers between devices  5.73 us (3%)
    pallas_call x1, Pallas kernels, expert_layer(): pl.pallas_call(functools.partial(expert_kernel, groups, capacity, halves)...  158 us
    pallas_call x3, Pallas kernels, exchange(): pl.pallas_call(functools.partial(exchange_kernel, axis, group, count, kin...  26 us
    unnamed x20, local copies, waits for them, and re-layouts  5.82 us
    ppermute x2, starting transfers between devices, to_group(): return lax.ppermute(value, 'sp', pairs)  5.22 us
    dot_general x2, matrix products, body(): jnp.dot(token_heads[c], out_proj[c * features:(c + 1) * features], prefer...  4.42 us
  transfers between devices with their start and end apart: 5, of which 0 were waited for; matrix products, arithmetic and copies ran while one was open for 11% of the time, Pallas kernels for 12%

profile of v3, /device:TPU:0, one launch (start us, length us, event | category | flops | bytes accessed | tf_op | source)
XLA Modules:
  0.0 219.8 jit_solution(4746851925875025742)
XLA Ops:
  0.0 0.8 copy.70
  0.8 5.1 %collective-permute-start = (s32[256,2]{1,0:T(8,128)S(1)}, s32[256,2]{1,0:T(8,128)S(1)}, u32[]{:S(2)}, u32[]{:S(2)}) collective-permute-start(s32[256,2]{1,0:T(8,128)S(1)} %copy.70), channel_id=1, source_target_pairs={{0,24},{2,26},{4,28},{6,30},{8,16},{10,18},{12,20},{14,22},{16,8},... | collective-permute-start | bytes 6152 | tf_op jit(solution)/shard_map/ppermute | solution.py:431
  6.0 0.1 collective-permute-start.1
  6.1 0.0 collective-permute-start.2
  6.1 0.5 collective-permute-start.3
  6.6 0.0 collective-permute-start.4
  6.6 0.1 iota_compare_fusion.3
  6.7 0.0 copy-start.4
  6.7 0.8 fusion.54
  7.5 0.7 fusion.46
  8.2 0.1 reshape.693
  8.3 0.4 reduce_window_sum.22
  8.7 0.1 slice.103
  8.8 0.2 subtract_reduce_fusion
  9.0 0.1 broadcast_add_fusion
  9.0 0.1 add.175
  9.1 0.2 slice_reduce_fusion.4
  9.3 1.3 copy.74
  10.6 1.1 copy.73
  11.7 0.2 fusion.52
  11.9 0.1 multiply_bitcast_fusion
  11.9 0.2 scatter.9.refs_1_
  12.2 1.0 convolution_convert_fusion.1
  13.1 11.7 %shard_map.136 = (bf16[16,16,256]{2,1,0:T(8,128)(2,1)}, f32[16,8,128]{2,1,0:T(8,128)}) custom-call(bf16[16,16,256]{2,1,0:T(8,128)(2,1)} %bitcast.82, f32[8,128]{1,0:T(8,128)} %copy-done.5), custom_call_target="tpu_custom_call" | custom-call | bytes 10000000 | tf_op jit(solution)/shard_map/pallas_call | solution.py:54
  24.8 0.9 fusion.53
  25.7 0.1 copy.62
  25.8 0.1 copy.63
  25.9 0.9 copy.76
  26.9 0.2 select_reduce_fusion
  27.0 0.1 fusion.51
  27.1 0.3 convolution_convert_fusion
  27.5 0.7 copy.77
  28.2 10.8 %shard_map.137 = bf16[16,16,256]{2,1,0:T(8,128)(2,1)} custom-call(bf16[16,16,256]{2,1,0:T(8,128)(2,1)} %bitcast.85), custom_call_target="tpu_custom_call" | custom-call | bytes 10000000 | tf_op jit(solution)/shard_map/pallas_call | solution.py:54
  39.0 0.2 dynamic-slice_reduce_fusion
  39.1 1.2 fusion.29
  40.4 0.5 fusion.8
  40.9 0.1 subtract_exponential_fusion
  41.0 2.1 fusion.13
  43.1 0.2 fusion.14
  43.3 0.0 copy-start.3
  43.4 0.3 copy.69
  43.7 0.7 copy-done.3
  44.4 1.1 multiply_convert_fusion.1
  45.5 3.5 %shard_map.138 = bf16[2,256,512]{2,1,0:T(8,128)(2,1)} custom-call(bf16[2,256,512]{2,1,0:T(8,128)(2,1)} %bitcast.79), custom_call_target="tpu_custom_call" | custom-call | bytes 2000000 | tf_op jit(solution)/shard_map/pallas_call | solution.py:54
  49.0 0.0 copy-start
  49.0 2.5 %fusion.6 = f32[256,2048]{1,0:T(8,128)S(1)} fusion(bf16[1024,2048]{1,0:T(8,128)(2,1)} %param.25, bf16[2,256,512]{2,1,0:T(8,128)(2,1)} %shard_map.138), kind=kOutput, calls=%fused_computation.10 | convolution fusion | flops 536870912 | bytes 4456448 | tf_op jit(solution)/shard_map/dot_general | solution.py:464
  51.5 0.3 copy-done
  51.9 1.9 fusion.2
  53.8 0.1 sub.97
  54.0 0.3 fusion.10
  54.3 0.1 convert_element_type.136
  54.5 1.3 fusion.4.refs_0_
  55.7 0.2 slice_reduce_fusion.3
  55.9 0.0 collective-permute-done
  56.0 0.1 sub.99
  56.1 0.3 fusion.11
  56.4 0.1 convert_element_type.142
  56.6 0.2 slice_reduce_fusion.1
  56.8 0.3 add_convert_fusion
  57.2 0.8 pad_maximum_fusion.1.refs_3_
  58.0 0.3 fusion.25
  58.3 0.9 pad_maximum_fusion.refs_2_
  59.2 158.3 %shard_map.139 = bf16[256,2048]{1,0:T(8,128)(2,1)} custom-call(bf16[256,2048]{1,0:T(8,128)(2,1)} %fusion.4.refs_0_, bf16[256,2048]{1,0:T(8,128)(2,1)} %copy-done.1, bf16[2,512,256]{2,1,0:T(8,128)(2,1)} %pad_maximum_fusion.refs_2_, bf16[2,256,512]{2,1,0:T(8,128)(2,1)} %pad_maximum_fusion.1.refs_3_, bf16[2048,384]{1,0:T(8,128)(2,1)} %bitcast.99, ...), custom_call_target="tpu_custom_call" | custom-call | flops 10000000000 | bytes 100000000 | tf_op jit(solution)/shard_map/pallas_call | solution.py:389
  217.5 2.3 %copy.91 = bf16[256,2048]{1,0:T(8,128)(2,1)} copy(bf16[256,2048]{1,0:T(8,128)(2,1)} %shard_map.139) | data formatting | bytes 2097152
  (30 shorter events, 0.2 us)
Async XLA Ops:
  0.0 11.7 %copy-start.7 = (f32[2,512]{1,0:T(2,128)S(1)}, f32[2,512]{1,0:T(2,128)}, u32[]{:S(2)}) copy-start(f32[2,512]{1,0:T(2,128)} %param.23) | copy-start | bytes 12292
  0.8 55.1 %collective-permute-start = (s32[256,2]{1,0:T(8,128)S(1)}, s32[256,2]{1,0:T(8,128)S(1)}, u32[]{:S(2)}, u32[]{:S(2)}) collective-permute-start(s32[256,2]{1,0:T(8,128)S(1)} %copy.70), channel_id=1, source_target_pairs={{0,24},{2,26},{4,28},{6,30},{8,16},{10,18},{12,20},{14,22},{16,8},... | collective-permute-start | bytes 6152 | tf_op jit(solution)/shard_map/ppermute | solution.py:431
  6.0 50.8 %collective-permute-start.1 = (f32[256,2]{0,1:T(2,128)}, f32[256,2]{0,1:T(2,128)S(1)}, u32[]{:S(2)}, u32[]{:S(2)}) collective-permute-start(f32[256,2]{0,1:T(2,128)} %param.31), channel_id=1, source_target_pairs={{0,24},{2,26},{4,28},{6,30},{8,16},{10,18},{12,20},{14,22},{16,8},... | collective-permute-start | bytes 6152 | tf_op jit(solution)/shard_map/ppermute | solution.py:431
  6.1 53.1 %collective-permute-start.2 = (bf16[2048,384]{1,0:T(8,128)(2,1)}, bf16[2048,384]{1,0:T(8,128)(2,1)}, u32[]{:S(2)}, u32[]{:S(2)}) collective-permute-start(bf16[2048,384]{1,0:T(8,128)(2,1)} %bitcast.98), channel_id=1, source_target_pairs={{0,1},{1,0},{2,3},{3,2},{4,5},{5,4},{6,7},{7,6},{8,9},{9,8},{10,11... | collective-permute-start | bytes 4718600 | tf_op jit(solution)/shard_map/ppermute | solution.py:434
  6.1 53.1 %collective-permute-start.3 = (bf16[2048,384]{1,0:T(8,128)(2,1)}, bf16[2048,384]{1,0:T(8,128)(2,1)}, u32[]{:S(2)}, u32[]{:S(2)}) collective-permute-start(bf16[2048,384]{1,0:T(8,128)(2,1)} %bitcast.100), channel_id=1, source_target_pairs={{0,1},{1,0},{2,3},{3,2},{4,5},{5,4},{6,7},{7,6},{8,9},{9,8},{10,11... | collective-permute-start | bytes 4718600 | tf_op jit(solution)/shard_map/ppermute | solution.py:434
  6.6 52.6 %collective-permute-start.4 = (bf16[384,2048]{1,0:T(8,128)(2,1)}, bf16[384,2048]{1,0:T(8,128)(2,1)}, u32[]{:S(2)}, u32[]{:S(2)}) collective-permute-start(bf16[384,2048]{1,0:T(8,128)(2,1)} %bitcast.102), channel_id=1, source_target_pairs={{0,1},{1,0},{2,3},{3,2},{4,5},{5,4},{6,7},{7,6},{8,9},{9,8},{10,11... | collective-permute-start | bytes 4718600 | tf_op jit(solution)/shard_map/ppermute | solution.py:434
  6.7 32.5 %copy-start.4 = (bf16[512,256]{1,0:T(8,128)(2,1)S(1)}, bf16[512,256]{1,0:T(8,128)(2,1)}, u32[]{:S(2)}) copy-start(bf16[512,256]{1,0:T(8,128)(2,1)} %param.19) | copy-start | bytes 786436
  12.1 1.0 copy-start.5
  43.3 1.0 copy-start.3
  45.5 6.1 %copy-start.2 = (bf16[256,2048]{1,0:T(8,128)(2,1)S(1)}, bf16[256,2048]{1,0:T(8,128)(2,1)}, u32[]{:S(2)}) copy-start(bf16[256,2048]{1,0:T(8,128)(2,1)} %param.18) | copy-start | bytes 3145732
  49.0 2.9 %copy-start = (bf16[1024,2048]{1,0:T(8,128)(2,1)S(1)}, bf16[1024,2048]{1,0:T(8,128)(2,1)}, u32[]{:S(2)}) copy-start(bf16[1024,2048]{1,0:T(8,128)(2,1)} %param.25) | copy-start | bytes 12582916
  51.9 2.6 %copy-start.6 = (f32[2048]{0:T(1024)S(1)}, f32[2048]{0:T(1024)}, u32[]{:S(2)}) copy-start(f32[2048]{0:T(1024)} %param.26) | copy-start | bytes 24580
  53.8 2.6 %copy-start.1 = (bf16[256,2048]{1,0:T(8,128)(2,1)}, bf16[256,2048]{1,0:T(8,128)(2,1)S(1)}, u32[]{:S(2)}) copy-start(bf16[256,2048]{1,0:T(8,128)(2,1)S(1)} %get-tuple-element.54.refs_1_) | copy-start | bytes 3145732
